TPU v7x, 32 devices: a whole 2x2x4 slice. The times are simulated.
32 devices in a mesh: sp: 8 (over z, y), tp: 4 (over x, core).
Axes of the slice: x: 2, y: 2, z: 4, core: 2. Of those that a mesh axis runs over, the one named last changes fastest.
Arguments:
- activations: bfloat16 [3584, 2048], P(('sp', 'tp')), may hold values from -27.5 to 27.5
- query_weight: bfloat16 [2048, 2048], P(None, 'tp'), may hold values from -0.088388348 to 0.088388348
- key_weight: bfloat16 [2048, 2048], P(None, 'tp'), may hold values from -0.088388348 to 0.088388348
- value_weight: bfloat16 [2048, 2048], P(None, 'tp'), may hold values from -0.125 to 0.125
- out_weight: bfloat16 [2048, 2048], P('tp'), may hold values from -0.125 to 0.125
- lambdas: float32 [8], P('tp'), may hold values from 0.3 to 0.8
- head_gain: float32 [256], replicated, may hold values from 0.1 to 1.9
Outputs:
- mixed: bfloat16 [3584, 2048], P(('sp', 'tp'))
All inputs are finite; a program needn't handle non-finite values.
Results may differ from a plain program's by a relative error of at most 0.014.
Values may be sent and summed in bfloat16 or wider, within the bound.
A program may use at most 128 MiB of HBM per device.

v0:
```python
import math

import jax
import jax.numpy as jnp
from jax import lax
from jax.sharding import PartitionSpec as P

HEAD = 128
VALUE = 256


norm_floor = 0.02
very_low = -1e30


def empty_state(count, local_heads):
    return (
        jnp.full((local_heads, 2, count), very_low, jnp.float32),
        jnp.zeros((local_heads, 2, count), jnp.float32),
        jnp.zeros((local_heads, 2, count, VALUE), jnp.float32),
    )


def absorb(state, query_set, query_pos, key_block, value_block, key_first):
    running, denoms, accums = state
    local_heads = running.shape[0]
    span = key_block.shape[0]
    key_grid = key_block.reshape(span, local_heads, 2, HEAD)
    scores = jnp.einsum(
        "qhme,khme->hmqk", query_set, key_grid, preferred_element_type=jnp.float32
    ) * HEAD ** (-0.5)
    key_pos = key_first + jnp.arange(span, dtype=jnp.int32)
    allowed = key_pos[None, :] <= query_pos[:, None]
    masked = jnp.where(allowed, scores, very_low)
    updated = jnp.maximum(running, jnp.max(masked, axis=-1))
    exp_weights = jnp.where(allowed, jnp.exp(masked - updated[..., None]), 0.0)
    factor = jnp.exp(running - updated)
    denoms = denoms * factor + jnp.sum(exp_weights, axis=-1)
    value_grid = value_block.reshape(span, local_heads, VALUE)
    product = jnp.einsum(
        "hmqk,khv->hmqv",
        exp_weights.astype(jnp.bfloat16),
        value_grid,
        preferred_element_type=jnp.float32,
    )
    accums = accums * factor[..., None] + product
    return (updated, denoms, accums)


def make_folder(query_sets, carry, pieces):
    key_piece, value_piece = pieces
    length = key_piece.shape[0]
    span = math.gcd(length, 512)

    def one_span(span_index, states):
        offset = span_index * span
        key_block = lax.dynamic_slice_in_dim(key_piece, offset, span, 0)
        value_block = lax.dynamic_slice_in_dim(value_piece, offset, span, 0)
        fresh = []
        for state, query_entry in zip(states, query_sets):
            query_set, query_pos = query_entry

            def take(current):
                return absorb(current, query_set, query_pos, key_block, value_block, offset)

            def leave(current):
                return current

            fresh.append(lax.cond(offset <= query_pos[-1], take, leave, state))
        return tuple(fresh)

    return lax.fori_loop(0, length // span, one_span, carry)


def shards(activations, query_weight, key_weight, value_weight, out_weight, lambdas, head_gain):
    local_heads = lambdas.shape[0]
    query_width = query_weight.shape[1]
    joined_weight = jnp.concatenate([query_weight, key_weight, value_weight], axis=1)
    projected = jnp.dot(
        lax.all_gather(activations, "tp", axis=0, tiled=True),
        joined_weight,
        preferred_element_type=jnp.float32,
    ).astype(jnp.bfloat16)
    row_count = projected.shape[0]
    queries = projected[:, :query_width].reshape(row_count, local_heads, 2, HEAD)
    key_rows = projected[:, query_width : 2 * query_width]
    value_rows = projected[:, 2 * query_width :]
    position = lax.axis_index("sp") * row_count + jnp.arange(row_count, dtype=jnp.int32)
    query_sets = [(queries, position)]
    start_states = tuple((empty_state(entry[0].shape[0], local_heads) for entry in query_sets))
    finals = make_folder(
        query_sets,
        start_states,
        (
            lax.all_gather(key_rows, "sp", axis=0, tiled=True),
            lax.all_gather(value_rows, "sp", axis=0, tiled=True),
        ),
    )
    outputs = []
    for state in finals:
        running, denoms, accums = state
        combined = (
            accums[:, 0] / denoms[:, 0, :, None]
            - lambdas[:, None, None] * accums[:, 1] / denoms[:, 1, :, None]
        )
        inverse_rms = lax.rsqrt(jnp.mean(combined * combined, axis=-1, keepdims=True) + norm_floor)
        normed = (combined * inverse_rms * head_gain).astype(jnp.bfloat16)
        outputs.append(
            jnp.transpose(normed, (1, 0, 2)).reshape(normed.shape[1], local_heads * VALUE)
        )
    heads_out = outputs[0]
    return lax.psum_scatter(
        jnp.dot(heads_out, out_weight, preferred_element_type=jnp.float32).astype(jnp.bfloat16),
        "tp",
        scatter_dimension=0,
        tiled=True,
    )


def solution(mesh):
    in_specs = (
        P(("sp", "tp"), None),
        P(None, "tp"),
        P(None, "tp"),
        P(None, "tp"),
        P("tp", None),
        P("tp"),
        P(),
    )
    out_specs = P(("sp", "tp"), None)
    return jax.shard_map(shards, mesh=mesh, in_specs=in_specs, out_specs=out_specs, check_vma=False)
```

profile of v0, /device:TPU:16, one launch (start us, length us, event | category | flops | bytes accessed | tf_op | source)
XLA Modules:
  0.0 275.2 jit_solution(14278011562459007727)
XLA Ops:
  7.3 23.8 %all-gather.4.cloned.1.call-done = bf16[448,2048]{1,0:T(8,128)(2,1)} async-done(((bf16[112,2048]{1,0:T(8,128)(2,1)}), bf16[448,2048]{1,0:T(8,128)(2,1)}) %all-gather.4.cloned.1.call-update) | async-done | bytes 1835024 | tf_op jit(solution)/shard_map/all_gather | solution.py:80
  31.1 6.4 %fusion.24 = bf16[448,1536]{1,0:T(8,128)(2,1)S(1)} fusion(bf16[448,2048]{1,0:T(8,128)(2,1)} %all-gather.4.cloned.1.call-done, bf16[2048,512]{1,0:T(8,128)(2,1)} %param.14, bf16[2048,512]{1,0:T(8,128)(2,1)} %param.13, bf16[2048,512]{1,0:T(8,128)(2,1)} %param.12), kind=kOutput, calls=%fused_computation.29 | convolution fusion | flops 2838134784 | bytes 9502720 | tf_op jit(solution)/shard_map/dot_general | solution.py:79
  39.5 65.0 %all-gather.8.cloned.1.call-done = bf16[3584,512]{1,0:T(8,128)(2,1)} async-done(((bf16[448,512]{1,0:T(8,128)(2,1)}), bf16[3584,512]{1,0:T(8,128)(2,1)}) %all-gather.8.cloned.1.call-update) | async-done | bytes 3670032 | tf_op jit(solution)/shard_map/all_gather | solution.py:96
  104.6 6.0 %copy.14 = bf16[3584,512]{0,1:T(8,128)(2,1)} copy(bf16[3584,512]{1,0:T(8,128)(2,1)} %all-gather.8.cloned.1.call-done) | data formatting | bytes 7340032 | tf_op jit(solution)/shard_map/while | solution.py:72
  110.5 61.2 %all-gather.6.cloned.1.call-done = bf16[3584,512]{1,0:T(8,128)(2,1)} async-done(((bf16[448,512]{1,0:T(8,128)(2,1)}), bf16[3584,512]{1,0:T(8,128)(2,1)}) %all-gather.6.cloned.1.call-update) | async-done | bytes 3670032 | tf_op jit(solution)/shard_map/all_gather | solution.py:95
  171.7 5.9 %copy.12 = bf16[3584,512]{0,1:T(8,128)(2,1)} copy(bf16[3584,512]{1,0:T(8,128)(2,1)} %all-gather.6.cloned.1.call-done) | data formatting | bytes 7340032 | tf_op jit(solution)/shard_map/while | solution.py:72
  177.7 1.5 broadcast_in_dim.39
  179.1 42.7 %while.17 = (s32[]{:T(128)}, f32[2,2,448]{2,1,0:T(2,128)S(1)}, f32[2,2,448]{2,1,0:T(2,128)S(1)}, f32[2,2,448,256]{3,2,1,0:T(8,128)}, s32[448]{0:T(512)S(1)}, /*i...) while((s32[]{:T(128)}, f32[2,2,448]{2,1,0:T(2,128)S(1)}, ...), condition=%wide.region_5.6_spmd, body=%wide.region_0.5_spmd.sunk | while | flops 717721600 | bytes 34003040 | solution.py:72
  180.5 6.7 %conditional.2 = ((f32[2,2,448]{2,1,0:T(2,128)S(1)}, f32[2,2,448]{2,1,0:T(2,128)S(1)}, f32[2,2,448,256]{3,2,1,0:T(8,128)})) conditional(s32[]{:T(128)} %convert_element_type.41, (f32[2,2,448]{2,1,0:T(2,128)S(1)}, f32[2,2,448]{2,1,0:T(2,128)S(1)}, f32[2,2,448,256]{3,2,1,0:T(8,128)}) %tuple.56, (s32[]{:T(128)}, s32[448]{0:T(512)S(1)}, ...), branch_computations={%region_1.0_spmd, %region_2.4_spmd} | conditional | flops 717721600 | bytes 34002816 | solution.py:69
  180.7 1.3 constant_dynamic-slice_fusion
  182.9 1.4 fusion.2
  184.3 1.5 multiply_add_fusion
  185.8 1.3 copy-done.2
  188.5 6.7 %conditional.2 = ((f32[2,2,448]{2,1,0:T(2,128)S(1)}, f32[2,2,448]{2,1,0:T(2,128)S(1)}, f32[2,2,448,256]{3,2,1,0:T(8,128)})) conditional(s32[]{:T(128)} %convert_element_type.41, (f32[2,2,448]{2,1,0:T(2,128)S(1)}, f32[2,2,448]{2,1,0:T(2,128)S(1)}, f32[2,2,448,256]{3,2,1,0:T(8,128)}) %tuple.56, (s32[]{:T(128)}, s32[448]{0:T(512)S(1)}, ...), branch_computations={%region_1.0_spmd, %region_2.4_spmd} | conditional | flops 717721600 | bytes 34002816 | solution.py:69
  190.9 1.4 fusion.2
  192.3 1.5 multiply_add_fusion
  193.8 1.3 copy-done.2
  196.5 6.7 %conditional.2 = ((f32[2,2,448]{2,1,0:T(2,128)S(1)}, f32[2,2,448]{2,1,0:T(2,128)S(1)}, f32[2,2,448,256]{3,2,1,0:T(8,128)})) conditional(s32[]{:T(128)} %convert_element_type.41, (f32[2,2,448]{2,1,0:T(2,128)S(1)}, f32[2,2,448]{2,1,0:T(2,128)S(1)}, f32[2,2,448,256]{3,2,1,0:T(8,128)}) %tuple.56, (s32[]{:T(128)}, s32[448]{0:T(512)S(1)}, ...), branch_computations={%region_1.0_spmd, %region_2.4_spmd} | conditional | flops 717721600 | bytes 34002816 | solution.py:69
  198.9 1.4 fusion.2
  200.3 1.5 multiply_add_fusion
  201.8 1.3 copy-done.2
  204.5 6.7 %conditional.2 = ((f32[2,2,448]{2,1,0:T(2,128)S(1)}, f32[2,2,448]{2,1,0:T(2,128)S(1)}, f32[2,2,448,256]{3,2,1,0:T(8,128)})) conditional(s32[]{:T(128)} %convert_element_type.41, (f32[2,2,448]{2,1,0:T(2,128)S(1)}, f32[2,2,448]{2,1,0:T(2,128)S(1)}, f32[2,2,448,256]{3,2,1,0:T(8,128)}) %tuple.56, (s32[]{:T(128)}, s32[448]{0:T(512)S(1)}, ...), branch_computations={%region_1.0_spmd, %region_2.4_spmd} | conditional | flops 717721600 | bytes 34002816 | solution.py:69
  206.9 1.4 fusion.2
  208.3 1.5 multiply_add_fusion
  209.8 1.3 copy-done.2
  212.5 6.7 %conditional.2 = ((f32[2,2,448]{2,1,0:T(2,128)S(1)}, f32[2,2,448]{2,1,0:T(2,128)S(1)}, f32[2,2,448,256]{3,2,1,0:T(8,128)})) conditional(s32[]{:T(128)} %convert_element_type.41, (f32[2,2,448]{2,1,0:T(2,128)S(1)}, f32[2,2,448]{2,1,0:T(2,128)S(1)}, f32[2,2,448,256]{3,2,1,0:T(8,128)}) %tuple.56, (s32[]{:T(128)}, s32[448]{0:T(512)S(1)}, ...), branch_computations={%region_1.0_spmd, %region_2.4_spmd} | conditional | flops 717721600 | bytes 34002816 | solution.py:69
  214.9 1.4 fusion.2
  216.3 1.5 multiply_add_fusion
  217.8 1.3 copy-done.2
  221.9 1.9 multiply_reduce_fusion
  224.1 2.4 convolution_convert_fusion
  226.6 42.1 %reduce-scatter.2.cloned.1.call-done = bf16[112,2048]{1,0:T(8,128)(2,1)} async-done(((bf16[448,2048]{1,0:T(8,128)(2,1)}), bf16[112,2048]{1,0:T(8,128)(2,1)}) %reduce-scatter.2.cloned.1.call-update) | async-done | bytes 458768 | tf_op jit(solution)/shard_map/reduce_scatter | solution.py:112
  (83 shorter events, 18.3 us)
Async XLA Ops:
  6.5 217.6 %copy-start = (bf16[512,2048]{1,0:T(8,128)(2,1)S(1)}, bf16[512,2048]{1,0:T(8,128)(2,1)}, u32[]{:S(2)}) copy-start(bf16[512,2048]{1,0:T(8,128)(2,1)} %param.15) | copy-start | bytes 6291460
  6.5 24.5 %all-gather.4.cloned.1.call-start = ((), (), s32[]{:S(2)}) async-start(), calls=%async_computation.1 | async-start | bytes 2293760 | tf_op jit(solution)/shard_map/all_gather | solution.py:80
  7.3 97.3 %all-gather.8.cloned.1.call-start = ((), (), s32[]{:S(2)}) async-start(), calls=%async_computation.3 | async-start | bytes 4128768 | tf_op jit(solution)/shard_map/all_gather | solution.py:96
  38.6 133.2 %all-gather.6.cloned.1.call-start = ((), (), s32[]{:S(2)}) async-start(), calls=%async_computation.2 | async-start | bytes 4128768 | tf_op jit(solution)/shard_map/all_gather | solution.py:95
  39.3 229.4 %reduce-scatter.2.cloned.1.call-start = ((), (), s32[]{:S(2)}) async-start(), calls=%async_computation.4 | async-start | bytes 2293760 | tf_op jit(solution)/shard_map/reduce_scatter | solution.py:112
  179.1 42.8 %copy-start.4 = (f32[2]{0:T(128)S(1)}, f32[2]{0:T(128)}, u32[]{:S(2)}) copy-start(f32[2]{0:T(128)} %param.16) | copy-start | bytes 28
  179.1 44.7 %copy-start.3 = (f32[256]{0:T(256)S(1)}, f32[256]{0:T(256)}, u32[]{:S(2)}) copy-start(f32[256]{0:T(256)} %param.17) | copy-start | bytes 3076
  182.0 2.3 copy-start.1
  185.8 1.3 copy-start.2
  190.0 2.3 copy-start.1
  193.8 1.3 copy-start.2
  198.0 2.3 copy-start.1
  201.8 1.3 copy-start.2
  206.0 2.3 copy-start.1
  209.8 1.3 copy-start.2
  214.0 2.3 copy-start.1
  217.8 1.3 copy-start.2
Sparse Core Ops, SparseCore 0:
  8.9 22.1 all-gather.3
  38.7 65.8 all-gather.7
  106.8 64.9 all-gather.5
  226.7 41.9 reduce-scatter.1
where the time goes:
time: 277 us; the launch traced here: 275 us
  waiting for transfers between devices  193 us (70%)
  local copies, waits for them, and re-layouts  32.1 us (12%)
  matrix products  20.6 us (7%)
  between operations  13.2 us (5%)
  other arithmetic  10.4 us (4%)
  loops' own time  5.22 us (2%)
    all_gather x1, waiting for transfers between devices, shards(): lax.all_gather(value_rows, 'sp', axis=0, tiled=True)  65 us
    all_gather x1, waiting for transfers between devices, shards(): lax.all_gather(key_rows, 'sp', axis=0, tiled=True)  61.2 us
    reduce_scatter x1, waiting for transfers between devices, shards(): lax.psum_scatter(jnp.dot(heads_out, out_weight, preferred_element_type=jn...  42.1 us
    all_gather x1, waiting for transfers between devices, shards(): lax.all_gather(activations, 'tp', axis=0, tiled=True)  23.8 us
    while x3, local copies, waits for them, and re-layouts, make_folder(): return lax.fori_loop(0, length // span, one_span, carry)  12 us
    dot_general x5, matrix products, absorb(): jnp.einsum('hmqk,khv->hmqv', exp_weights.astype(jnp.bfloat16), value_grid...  7.46 us
    reduce_sum x5, other arithmetic, absorb(): denoms = denoms * factor + jnp.sum(exp_weights, axis=-1)  7.09 us
    cond x25, local copies, waits for them, and re-layouts  6.52 us
  transfers between devices with their start and end apart: 4, of which 4 were waited for; matrix products, arithmetic and copies ran while one was open for 2% of the time, Pallas kernels for 0%

commit v1 on v0

--- a/solution.py
+++ b/solution.py
@@ -1,8 +1,11 @@
+import functools
 import math
 
 import jax
 import jax.numpy as jnp
 from jax import lax
+from jax.experimental import pallas as pl
+from jax.experimental.pallas import tpu as pltpu
 from jax.sharding import PartitionSpec as P
 
 HEAD = 128
@@ -11,6 +14,385 @@
 
 norm_floor = 0.02
 very_low = -1e30
+MESH = pl.DeviceIdType.MESH
+
+
+def layer_kernel(
+    S, T, L, R,
+    act, qw, kw, vw, ow, lam_in, gain,
+    out,
+    A, WP, W, PR, PC, KV, HO, HI, LB, ACC, MX, DN, TOT,
+    w_sem, own_sem, a_send, a_recv, lam_send, lam_recv, o_send, o_recv,
+    p_send, p_recv, f_send, f_recv, h_send, h_recv,
+):
+    X = T // 2
+    half = T // 2
+    s = lax.axis_index("sp")
+    t = lax.axis_index("tp")
+    x = t // 2
+    c = t % 2
+    mate = x * 2 + (1 - c)
+    hl = s // half
+    r = (s % half) * 2 + c
+    head = x * 2 * L + hl
+    width = L * 256
+
+    def remote(src, dst, ss, rs, sp, tp):
+        return pltpu.make_async_remote_copy(
+            src_ref=src, dst_ref=dst, send_sem=ss, recv_sem=rs,
+            device_id=(sp, tp), device_id_type=MESH,
+        )
+
+    def weight_copies():
+        return [
+            pltpu.make_async_copy(ref, WP.at[k], w_sem.at[k])
+            for k, ref in enumerate((qw, kw, vw))
+        ]
+
+    def own_copies():
+        return [
+            pltpu.make_async_copy(act, A.at[t], own_sem.at[0]),
+            pltpu.make_async_copy(ow, W.at[pl.ds(t * L, L)], own_sem.at[1]),
+            pltpu.make_async_copy(lam_in, LB.at[c], own_sem.at[2]),
+        ]
+
+    def act_out(k):
+        if k == 0:
+            return remote(act, A.at[t], a_send.at[0], a_recv.at[t], s, mate)
+        return remote(act, A.at[t], a_send.at[k], a_recv.at[t], s, ((x + k) % X) * 2 + c)
+
+    def act_pass(k):
+        src = ((x + k) % X) * 2 + c
+        return remote(A.at[src], A.at[src], a_send.at[X - 1 + k], a_recv.at[src], s, mate)
+
+    def ow_part(i):
+        return pl.ds(i * L, L)
+
+    def ow_out(k):
+        dst = mate if k == 0 else ((x + k) % X) * 2 + c
+        return remote(ow, W.at[ow_part(t)], o_send.at[k], o_recv.at[t], s, dst)
+
+    def ow_pass(k):
+        src = ((x + k) % X) * 2 + c
+        return remote(
+            W.at[ow_part(src)], W.at[ow_part(src)],
+            o_send.at[X - 1 + k], o_recv.at[src], s, mate,
+        )
+
+    lam_out = remote(lam_in, LB.at[c], lam_send.at[0], lam_recv.at[0], s, mate)
+
+    for k in range(1, X):
+        act_out(k).start()
+    act_out(0).start()
+    for copy in weight_copies():
+        copy.start()
+    for copy in own_copies():
+        copy.start()
+    lam_out.start()
+    for k in range(1, X):
+        ow_out(k).start()
+    ow_out(0).start()
+
+    def piece_place(l, q):
+        return (c * L + l) * half + q // 2, x * 2 + q % 2
+
+    def piece(l, q):
+        sp, tp = piece_place(l, q)
+        return remote(
+            PR.at[l, q], PC.at[s], p_send.at[l, q], p_recv.at[s], sp, tp
+        )
+
+    def piece_here(l, q):
+        return pltpu.make_async_copy(PR.at[l, q], PC.at[s], p_recv.at[s])
+
+    def send_piece(l, q):
+        sp, tp = piece_place(l, q)
+        here = (sp == s) & (tp == t)
+
+        @pl.when(here)
+        def _():
+            piece_here(l, q).start()
+
+        @pl.when(jnp.logical_not(here))
+        def _():
+            piece(l, q).start()
+
+    def project(k, carry):
+        xx = (x + k) % X
+        rows = A[pl.ds(xx * 2, 2)].reshape(2 * R, A.shape[2])
+        for part in range(3):
+            got = jnp.dot(rows, WP[part], preferred_element_type=jnp.float32)
+            got = got.astype(jnp.bfloat16)
+            for l in range(L):
+                cols = got[:, l * 256:(l + 1) * 256]
+                PR[l, pl.ds(xx * 2, 2), :, part * 256:(part + 1) * 256] = cols.reshape(2, R, 256)
+        for l in range(L):
+            for q in range(2):
+                send_piece(l, xx * 2 + q)
+        return carry
+
+    def wait_act(i):
+        remote(act, A.at[i], a_send.at[0], a_recv.at[i], s, mate).wait_recv()
+
+    own_copies()[0].wait()
+    for copy in weight_copies():
+        copy.wait()
+    wait_act(mate)
+    project(0, 0)
+    for k in range(1, X):
+        wait_act(((x + k) % X) * 2 + c)
+        act_pass(k).start()
+        wait_act(((x + k) % X) * 2 + (1 - c))
+        project(k, 0)
+
+    span = T * R
+
+    def kv_row(block, member):
+        return pl.ds(block * span + member * R, R)
+
+    def kv_copy(kind, block, member, src, sp, tp):
+        return remote(
+            src, KV.at[kv_row(block, member)],
+            f_send.at[kind, block], f_recv.at[block, member], sp, tp,
+        )
+
+    def on_chip_row(y):
+        return hl * half + y
+
+    y = s % half
+
+    def spread_own(block):
+        return [
+            kv_copy(0, block, r, PC.at[block, :, 256:768], s, mate)
+        ] + [
+            kv_copy(k, block, r, PC.at[block, :, 256:768], on_chip_row((y + k) % half), t)
+            for k in range(1, half)
+        ]
+
+    def pass_on(block, k):
+        member = ((y + k) % half) * 2 + c
+        return kv_copy(
+            half - 1 + k, block, member, KV.at[kv_row(block, member)], s, mate
+        )
+
+    def kv_here(block):
+        return pltpu.make_async_copy(
+            PC.at[block, :, 256:768], KV.at[kv_row(block, r)], f_recv.at[block, r]
+        )
+
+    def wait_kv(block, member):
+        kv_copy(0, block, member, PC.at[block, :, 256:768], s, mate).wait_recv()
+
+    def wait_piece(block):
+        remote(PR.at[0, 0], PC.at[block], p_send.at[0, 0], p_recv.at[block], s, mate).wait_recv()
+
+    def order(i):
+        return (hl * half + i) % S
+
+    def forward(i, carry):
+        block = order(i)
+        wait_piece(block)
+        for copy in spread_own(block)[::-1]:
+            copy.start()
+        kv_here(block).start()
+        return carry
+
+    def relay(i, carry):
+        block = order(i)
+        for k in range(1, half):
+            wait_kv(block, ((y + k) % half) * 2 + c)
+            pass_on(block, k).start()
+        return carry
+
+    def both(i, carry):
+        forward(i, carry)
+
+        @pl.when(i > 0)
+        def _():
+            relay(i - 1, carry)
+
+        return carry
+
+    lax.fori_loop(0, S, both, 0)
+    relay(S - 1, 0)
+
+    own_copies()[2].wait()
+    lam_out.wait_recv()
+    pair = 2
+    q_rows = pair * R
+    k_rows = pair * span
+    scale = HEAD ** (-0.5) * math.log2(math.e)
+
+    def wait_block(block):
+        kv_here(block).wait()
+        for k in range(half):
+            if k > 0:
+                pass
+            wait_kv(block, ((y + k) % half) * 2 + (1 - c))
+
+    def home(block):
+        return remote(
+            HO.at[block], HI.at[head], h_send.at[block], h_recv.at[head], block, r
+        )
+
+    def home_here(block):
+        return pltpu.make_async_copy(HO.at[block], HI.at[head], h_recv.at[head])
+
+    def chunk(i, j, masked):
+        for m in range(2):
+            q = PC[pl.ds(i * pair, pair), :, m * 128:(m + 1) * 128].reshape(q_rows, 128)
+            keys = KV[pl.ds(j * k_rows, k_rows), m * 128:(m + 1) * 128]
+            sc = lax.dot_general(
+                q, keys, (((1,), (1,)), ((), ())), preferred_element_type=jnp.float32
+            ) * scale
+            if masked:
+                row = lax.broadcasted_iota(jnp.int32, (q_rows, k_rows), 0)
+                col = lax.broadcasted_iota(jnp.int32, (q_rows, k_rows), 1)
+                pos = row + r * R
+                for b in range(1, pair):
+                    pos = pos + jnp.where(row >= b * R, span - R, 0)
+                sc = jnp.where(col <= pos, sc, very_low)
+            old = MX[m, :, :1]
+            new = jnp.maximum(old, jnp.max(sc, axis=1, keepdims=True))
+            p = jnp.exp2(sc - new)
+            factor = jnp.exp2(old - new)
+            total = DN[m, :, :1] * factor + jnp.sum(p, axis=1, keepdims=True)
+            values = KV[pl.ds(j * k_rows, k_rows), 256:512]
+            got = jnp.dot(p.astype(jnp.bfloat16), values, preferred_element_type=jnp.float32)
+            ACC[m] = ACC[m] * factor + got
+            MX[m] = jnp.broadcast_to(new, MX.shape[1:])
+            DN[m] = jnp.broadcast_to(total, DN.shape[1:])
+
+    lam = LB[hl // L, hl % L][:1, :1]
+
+    def tile(i, carry):
+        for b in range(pair):
+            wait_block(i * pair + b)
+        MX[...] = jnp.full(MX.shape, very_low, jnp.float32)
+        DN[...] = jnp.zeros(DN.shape, jnp.float32)
+        ACC[...] = jnp.zeros(ACC.shape, jnp.float32)
+
+        def inner(j, carry2):
+            chunk(i, j, False)
+            return carry2
+
+        lax.fori_loop(0, i, inner, 0)
+        chunk(i, i, True)
+        comb = ACC[0] / DN[0, :, :1] - lam * (ACC[1] / DN[1, :, :1])
+        inv = lax.rsqrt(jnp.mean(comb * comb, axis=1, keepdims=True) + norm_floor)
+        normed = (comb * inv * gain[...]).astype(jnp.bfloat16)
+        HO[pl.ds(i * pair, pair)] = normed.reshape(pair, R, 256)
+        for b in range(pair):
+            block = i * pair + b
+            here = (block == s) & (r == t)
+
+            @pl.when(here)
+            def _():
+                home_here(block).start()
+
+            @pl.when(jnp.logical_not(here))
+            def _():
+                home(block).start()
+
+        return carry
+
+    lax.fori_loop(0, S // pair, tile, 0)
+
+    def wait_ow(i):
+        remote(ow, W.at[ow_part(i)], o_send.at[0], o_recv.at[i], s, mate).wait_recv()
+
+    own_copies()[1].wait()
+    for k in range(1, X):
+        wait_ow(((x + k) % X) * 2 + c)
+        ow_pass(k).start()
+    wait_ow(mate)
+    for k in range(1, X):
+        wait_ow(((x + k) % X) * 2 + (1 - c))
+
+    TOT[...] = jnp.zeros(TOT.shape, jnp.float32)
+
+    def add_head(i, carry):
+        remote(HO.at[0], HI.at[i], h_send.at[0], h_recv.at[i], s, mate).wait_recv()
+        TOT[...] += jnp.dot(HI[i], W[i], preferred_element_type=jnp.float32)
+        return carry
+
+    lax.fori_loop(0, T * L, add_head, 0)
+    out[...] = TOT[...].astype(jnp.bfloat16)
+
+    lam_out.wait_send()
+    for k in range(X):
+        act_out(k).wait_send()
+        ow_out(k).wait_send()
+    for k in range(1, X):
+        act_pass(k).wait_send()
+        ow_pass(k).wait_send()
+    for l in range(L):
+        for q in range(T):
+            sp, tp = piece_place(l, q)
+
+            @pl.when(jnp.logical_not((sp == s) & (tp == t)))
+            def _():
+                piece(l, q).wait_send()
+
+    def drain(block, carry):
+        for copy in spread_own(block):
+            copy.wait_send()
+        for k in range(1, half):
+            pass_on(block, k).wait_send()
+
+        @pl.when(jnp.logical_not((block == s) & (r == t)))
+        def _():
+            home(block).wait_send()
+
+        return carry
+
+    lax.fori_loop(0, S, drain, 0)
+
+
+def fused(S, T, L, activations, query_weight, key_weight, value_weight, out_weight, lambdas, head_gain):
+    R, D = activations.shape
+    X = T // 2
+    half = T // 2
+    bf, f32 = jnp.bfloat16, jnp.float32
+    vmem = pl.BlockSpec(memory_space=pltpu.VMEM)
+    hbm = pl.BlockSpec(memory_space=pl.ANY)
+    dma = pltpu.SemaphoreType.DMA
+    lam_in = jnp.broadcast_to(lambdas[:, None, None], (L, 8, 128))
+    width = query_weight.shape[1]
+    return pl.pallas_call(
+        functools.partial(layer_kernel, S, T, L, R),
+        out_shape=jax.ShapeDtypeStruct((R, D), bf),
+        in_specs=[vmem, hbm, hbm, hbm, hbm, vmem, vmem],
+        out_specs=vmem,
+        scratch_shapes=[
+            pltpu.VMEM((T, R, D), bf),
+            pltpu.VMEM((3, D, width), bf),
+            pltpu.VMEM((T * L, VALUE, D), bf),
+            pltpu.VMEM((L, T, R, 768), bf),
+            pltpu.VMEM((S, R, 768), bf),
+            pltpu.VMEM((S * T * R, 512), bf),
+            pltpu.VMEM((S, R, VALUE), bf),
+            pltpu.VMEM((T * L, R, VALUE), bf),
+            pltpu.VMEM((2, L, 8, 128), f32),
+            pltpu.VMEM((2, 2 * R, VALUE), f32),
+            pltpu.VMEM((2, 2 * R, 128), f32),
+            pltpu.VMEM((2, 2 * R, 128), f32),
+            pltpu.VMEM((R, D), f32),
+            dma((3,)), dma((3,)),
+            dma((2 * X - 1,)), dma((T,)),
+            dma((1,)), dma((1,)),
+            dma((2 * X - 1,)), dma((T,)),
+            dma((L, T)), dma((S,)),
+            dma((2 * half - 1, S)), dma((S, T)),
+            dma((S,)), dma((T * L,)),
+        ],
+        compiler_params=pltpu.CompilerParams(
+            has_side_effects=True, vmem_limit_bytes=60 * 1024 * 1024
+        ),
+    )(
+        activations, query_weight, key_weight, value_weight,
+        out_weight.reshape(L, VALUE, D), lam_in, head_gain.reshape(1, VALUE),
+    )
 
 
 def empty_state(count, local_heads):
@@ -128,4 +510,15 @@
         P(),
     )
     out_specs = P(("sp", "tp"), None)
-    return jax.shard_map(shards, mesh=mesh, in_specs=in_specs, out_specs=out_specs, check_vma=False)
+    S, T = mesh.shape["sp"], mesh.shape["tp"]
+
+    def layer(*args):
+        L = args[5].shape[0] // T
+        rows = args[0].shape[0] // (S * T)
+        fits = T % 2 == 0 and S == L * T and S % 2 == 0 and rows % 16 == 0
+        local = functools.partial(fused, S, T, L) if fits else shards
+        return jax.shard_map(
+            local, mesh=mesh, in_specs=in_specs, out_specs=out_specs, check_vma=False
+        )(*args)
+
+    return layer

time: 277 us -> 88.7 us (0.32)
  the two profiles are of different devices: /device:TPU:16 before, /device:TPU:31 now
where the time goes in v1:
time: 88.7 us; the launch traced here: 88.5 us
  Pallas kernels  85.4 us (96%)
  local copies, waits for them, and re-layouts  3.14 us (4%)
    pallas_call x1, Pallas kernels, fused(): pl.pallas_call(functools.partial(layer_kernel, S, T, L, R), out_shape=jax...  85.4 us
    unnamed x1, local copies, waits for them, and re-layouts  1.82 us

profile of v1, /device:TPU:31, one launch (start us, length us, event | category | flops | bytes accessed | tf_op | source)
XLA Modules:
  0.0 88.5 jit_solution(13709836514010474679)
XLA Ops:
  0.0 1.3 %broadcast_in_dim.2.lam_in = f32[2,8,128]{2,1,0:T(8,128)} broadcast(f32[2]{0:T(128)} %param.12), dimensions={0} | broadcast | bytes 8200 | tf_op jit(solution)/shard_map/broadcast_in_dim | solution.py:360
  1.3 85.4 %shard_map.73 = bf16[112,2048]{1,0:T(8,128)(2,1)} custom-call(bf16[112,2048]{1,0:T(8,128)(2,1)} %act.1, bf16[2048,512]{1,0:T(8,128)(2,1)} %qw.1, bf16[2048,512]{1,0:T(8,128)(2,1)} %kw.1, bf16[2048,512]{1,0:T(8,128)(2,1)} %vw.1, bf16[2,256,2048]{2,1,0:T(8,128)(2,1)} %bitcast.2, f32[2,8,128]{2,1,0:T(8,128)} %broadcast_in_dim.2.lam_in, f32[1,256]{1,0:T(1,128)} %bitcast.3), custom_call_target="tpu_custom_call" | custom-call | tf_op jit(solution)/shard_map/pallas_call | solution.py:362
  86.7 1.8 %copy.9 = bf16[112,2048]{1,0:T(8,128)(2,1)} copy(bf16[112,2048]{1,0:T(8,128)(2,1)} %shard_map.73) | data formatting | bytes 917504

commit v2 on v0

--- a/solution.py
+++ b/solution.py
@@ -1,8 +1,11 @@
+import functools
 import math
 
 import jax
 import jax.numpy as jnp
 from jax import lax
+from jax.experimental import pallas as pl
+from jax.experimental.pallas import tpu as pltpu
 from jax.sharding import PartitionSpec as P
 
 HEAD = 128
@@ -11,6 +14,417 @@
 
 norm_floor = 0.02
 very_low = -1e30
+MESH = pl.DeviceIdType.MESH
+
+
+def layer_kernel(
+    S, T, L, R,
+    act, qw, kw, vw, ow, lam_in, gain,
+    out,
+    A, WP, W, PR, PC, KV, HO, HI, LS, LB, ACC, MX, DN, TOT,
+    w_sem, own_sem, a_send, a_recv, lam_send, lam_recv, o_send, o_recv, m_send, m_recv,
+    p_send, p_recv, f_send, f_recv, h_send, h_recv,
+):
+    X, Y = 2, 2
+    Z = S // Y
+    s = lax.axis_index("sp")
+    t = lax.axis_index("tp")
+    x = t // 2
+    c = t % 2
+    y = s % Y
+    z = s // Y
+    mate = x * 2 + (1 - c)
+    across = (1 - x) * 2 + c
+    beside = z * Y + (1 - y)
+    upper = z // (Z // 2)
+    near = upper * (Z // 2)
+    head = x * 2 * L + z
+    span = T * R
+    scale = HEAD ** (-0.5) * math.log2(math.e)
+
+    def remote(src, dst, ss, rs, sp, tp):
+        return pltpu.make_async_remote_copy(
+            src_ref=src, dst_ref=dst, send_sem=ss, recv_sem=rs,
+            device_id=(sp, tp), device_id_type=MESH,
+        )
+
+    def weight_copy(k):
+        return pltpu.make_async_copy((qw, kw, vw)[k], WP.at[k], w_sem.at[k])
+
+    def own_act():
+        return pltpu.make_async_copy(act, A.at[t], own_sem.at[0])
+
+    def own_ow():
+        return pltpu.make_async_copy(ow, W.at[pl.ds(t * L, L)], own_sem.at[1])
+
+    def act_across():
+        return remote(act, A.at[t], a_send.at[0], a_recv.at[t], s, across)
+
+    def act_mate():
+        return remote(act, A.at[t], a_send.at[1], a_recv.at[t], s, mate)
+
+    def act_pass():
+        return remote(A.at[across], A.at[across], a_send.at[2], a_recv.at[across], s, mate)
+
+    def wait_act(i):
+        remote(act, A.at[i], a_send.at[0], a_recv.at[i], s, mate).wait_recv()
+
+    def quarter(owner, q):
+        rows = pl.ds(pl.multiple_of((q % 2) * (VALUE // 2), VALUE // 2), VALUE // 2)
+        return owner * L + q // 2, rows
+
+    def turn(j, row):
+        return row * (2 * L - 1) if j == 0 else j
+
+    def ow_across(j):
+        q = turn(j, y)
+        place, rows = quarter(t, q)
+        return remote(
+            ow.at[q // 2, rows], W.at[place, rows], o_send.at[j], o_recv.at[j], s, across
+        )
+
+    def ow_mate():
+        return remote(ow, W.at[pl.ds(t * L, L)], m_send.at[0], m_recv.at[0], s, mate)
+
+    last = 2 * L - 1
+
+    def ow_beside():
+        place, rows = quarter(across, turn(0, y))
+        part = W.at[place, rows]
+        return remote(part, part, o_send.at[last], o_recv.at[last], beside, t)
+
+    def ow_pass(j):
+        q = turn(0, 1 - y) if j == last else turn(j, y)
+        place, rows = quarter(across, q)
+        part = W.at[place, rows]
+        return remote(part, part, m_send.at[1 + j], m_recv.at[1 + j], s, mate)
+
+    def lam_out():
+        return remote(LS, LB, lam_send.at[0], lam_recv.at[0], s, mate)
+
+    for l in range(L):
+        LS[l] = jnp.full((8, 128), lam_in[l], jnp.float32)
+    act_across().start()
+    act_mate().start()
+    for k in range(3):
+        weight_copy(k).start()
+    own_act().start()
+    for j in range(last):
+        ow_across(j).start()
+    own_ow().start()
+
+    def piece_sp(l):
+        return (c * L + l) * Y + y
+
+    def piece(l, xx, d):
+        return remote(
+            PR.at[l, xx, d], PC.at[z, xx], p_send.at[l, xx, d], p_recv.at[z, xx],
+            piece_sp(l), x * 2 + d,
+        )
+
+    def stays(l, d):
+        return (piece_sp(l) == s) & (c == d)
+
+    def send_piece(l, xx, d):
+        @pl.when(stays(l, d))
+        def _():
+            pltpu.make_async_copy(PR.at[l, xx, d], PC.at[z, xx], p_recv.at[z, xx]).start()
+
+        @pl.when(jnp.logical_not(stays(l, d)))
+        def _():
+            piece(l, xx, d).start()
+
+    def project(xx):
+        rows = A[pl.ds(xx * 2, 2)].reshape(2 * R, A.shape[2])
+        for part in range(3):
+            got = jnp.dot(rows, WP[part], preferred_element_type=jnp.float32)
+            if part == 0:
+                got = got * scale
+            got = got.astype(jnp.bfloat16)
+            for l in range(L):
+                cols = got[:, l * 256:(l + 1) * 256]
+                PR[l, xx, :, :, part * 256:(part + 1) * 256] = cols.reshape(2, R, 256)
+        for i in range(L):
+            l = upper * i + (1 - upper) * (L - 1 - i)
+            for d in range(2):
+                send_piece(l, xx, d)
+
+    own_act().wait()
+    for k in range(3):
+        weight_copy(k).wait()
+    wait_act(mate)
+    project(x)
+    ow_mate().start()
+    lam_out().start()
+    wait_act(across)
+    act_pass().start()
+    wait_act((1 - x) * 2 + (1 - c))
+    project(1 - x)
+
+    def kv_rows(row, zs, xx, core):
+        return pl.ds(((zs * Y + row) * T + xx * 2 + core) * R, R)
+
+    def kv_part(zs, xx):
+        return PC.at[zs, xx, :, 256:768]
+
+    def to_beside(zs, xx):
+        return remote(
+            kv_part(zs, xx), KV.at[kv_rows(y, zs, xx, c)],
+            f_send.at[0, zs, xx], f_recv.at[0, zs, xx], beside, t,
+        )
+
+    def to_mate(zs, xx):
+        return remote(
+            kv_part(zs, xx), KV.at[kv_rows(y, zs, xx, c)],
+            f_send.at[1, zs, xx], f_recv.at[1, zs, xx], s, mate,
+        )
+
+    def to_mate_again(zs, xx):
+        part = KV.at[kv_rows(1 - y, zs, xx, c)]
+        return remote(part, part, f_send.at[2, zs, xx], f_recv.at[2, zs, xx], s, mate)
+
+    def to_self(zs, xx):
+        return pltpu.make_async_copy(
+            kv_part(zs, xx), KV.at[kv_rows(y, zs, xx, c)], f_recv.at[3, zs, xx]
+        )
+
+    def place(i):
+        return (near + i // X) % Z, (x + i) % X
+
+    def forward(i):
+        zs, xx = place(i)
+        remote(PR.at[0, 0, 0], PC.at[zs, xx], p_send.at[0, 0, 0], p_recv.at[zs, xx], s, mate).wait_recv()
+        to_beside(zs, xx).start()
+        to_mate(zs, xx).start()
+        to_self(zs, xx).start()
+
+    def relay(i):
+        zs, xx = place(i)
+        to_beside(zs, xx).wait_recv()
+        to_mate_again(zs, xx).start()
+
+    def spread(first, count):
+        def both(i, carry):
+            forward(first + i)
+
+            @pl.when(i > 0)
+            def _():
+                relay(first + i - 1)
+
+            return carry
+
+        lax.fori_loop(0, count, both, 0)
+        relay(first + count - 1)
+
+    def wait_plane(zs):
+        for xx in range(X):
+            to_self(zs, xx).wait()
+            to_mate(zs, xx).wait_recv()
+            to_mate_again(zs, xx).wait_recv()
+
+    q_rows = X * R
+    k_rows = Y * span
+
+    def chunk(i, j, masked):
+        for m in range(2):
+            q = PC[i, :, :, m * 128:(m + 1) * 128].reshape(q_rows, 128)
+            keys = KV[pl.ds(j * k_rows, k_rows), m * 128:(m + 1) * 128]
+            sc = lax.dot_general(
+                q, keys, (((1,), (1,)), ((), ())), preferred_element_type=jnp.float32
+            )
+            if masked:
+                row = lax.broadcasted_iota(jnp.int32, (q_rows, 1), 0)
+                col = lax.broadcasted_iota(jnp.int32, (q_rows, k_rows), 1)
+                pos = row + jnp.where(row >= R, R, 0) + (y * span + c * R)
+                sc = jnp.where(col <= pos, sc, very_low)
+            old = MX[i, m, :, :1]
+            new = jnp.maximum(old, jnp.max(sc, axis=1, keepdims=True))
+            p = jnp.exp2(sc - new)
+            factor = jnp.exp2(old - new)
+            total = DN[i, m, :, :1] * factor + jnp.sum(p, axis=1, keepdims=True)
+            values = KV[pl.ds(j * k_rows, k_rows), 256:512]
+            got = jnp.dot(p.astype(jnp.bfloat16), values, preferred_element_type=jnp.float32)
+            ACC[i, m] = ACC[i, m] * factor + got
+            MX[i, m] = jnp.broadcast_to(new, MX.shape[2:])
+            DN[i, m] = jnp.broadcast_to(total, DN.shape[2:])
+
+    def chunks(i, low, high, diagonal):
+        def inner(j, carry):
+            chunk(i, j, False)
+            return carry
+
+        lax.fori_loop(low, high, inner, 0)
+
+        @pl.when(diagonal)
+        def _():
+            chunk(i, i, True)
+
+    def home(zs, xx):
+        return remote(
+            HO.at[zs, xx], HI.at[head], h_send.at[zs, xx], h_recv.at[head],
+            zs * Y + y, xx * 2 + c,
+        )
+
+    def ends_here(zs, xx):
+        return (zs == z) & (xx == x)
+
+    def finish(i):
+        mine = jnp.where(z // L == c, LS[z % L], LB[z % L])[:1, :1]
+        comb = ACC[i, 0] / DN[i, 0, :, :1] - mine * (ACC[i, 1] / DN[i, 1, :, :1])
+        inv = lax.rsqrt(jnp.mean(comb * comb, axis=1, keepdims=True) + norm_floor)
+        HO[i] = (comb * inv * gain[...]).astype(jnp.bfloat16).reshape(X, R, VALUE)
+        for k in range(X):
+            xx = (x + 1 + k) % X
+
+            @pl.when(ends_here(i, xx))
+            def _():
+                pltpu.make_async_copy(HO.at[i, xx], HI.at[head], h_recv.at[head]).start()
+
+            @pl.when(jnp.logical_not(ends_here(i, xx)))
+            def _():
+                home(i, xx).start()
+
+    MX[...] = jnp.full(MX.shape, very_low, jnp.float32)
+    DN[...] = jnp.zeros(DN.shape, jnp.float32)
+    ACC[...] = jnp.zeros(ACC.shape, jnp.float32)
+    H = Z // 2
+    spread(0, H * X)
+    ow_across(0).wait_recv()
+    ow_beside().start()
+    ow_pass(0).start()
+    lam_out().wait_recv()
+    for i in range(H):
+        wait_plane(near + i)
+
+    def step(k, carry):
+        @pl.when(k == H)
+        def _():
+            spread(H * X, H * X)
+            for i in range(H):
+                wait_plane((near + H + i) % Z)
+            for j in range(1, last - 1):
+                ow_across(j).wait_recv()
+                ow_pass(j).start()
+
+        early = k < H
+        i = jnp.where(early, near + k, jnp.where(upper == 1, k - H, Z - 1 - (k - H)))
+        partial = (upper == 1) & (i >= H)
+        low = jnp.where(early, near, 0)
+        high = jnp.where(partial & jnp.logical_not(early), H, i)
+        used = (upper == 1) | (k < Z)
+
+        @pl.when(used)
+        def _():
+            chunks(i, low, high, jnp.logical_not(partial) | early)
+
+            @pl.when(jnp.logical_not(partial & early))
+            def _():
+                finish(i)
+
+        return carry
+
+    lax.fori_loop(0, Z + H, step, 0)
+
+    own_ow().wait()
+    ow_mate().wait_recv()
+    ow_across(last - 1).wait_recv()
+    ow_pass(last - 1).start()
+    ow_beside().wait_recv()
+    ow_pass(last).start()
+    TOT[...] = jnp.zeros(TOT.shape, jnp.float32)
+
+    def add_head(i, carry):
+        @pl.when(i == 2 * L)
+        def _():
+            for j in range(last + 1):
+                ow_pass(j).wait_recv()
+
+        h = (x * 2 * L + i) % (T * L)
+        remote(HO.at[0, 0], HI.at[h], h_send.at[0, 0], h_recv.at[h], s, mate).wait_recv()
+        TOT[...] += jnp.dot(HI[h], W[h], preferred_element_type=jnp.float32)
+        return carry
+
+    lax.fori_loop(0, T * L, add_head, 0)
+    out[...] = TOT[...].astype(jnp.bfloat16)
+
+    act_across().wait_send()
+    act_mate().wait_send()
+    act_pass().wait_send()
+    ow_mate().wait_send()
+    ow_beside().wait_send()
+    for j in range(last):
+        ow_across(j).wait_send()
+    for j in range(last + 1):
+        ow_pass(j).wait_send()
+    lam_out().wait_send()
+    for l in range(L):
+        for xx in range(X):
+            for d in range(2):
+                @pl.when(jnp.logical_not(stays(l, d)))
+                def _():
+                    piece(l, xx, d).wait_send()
+
+    def drain(zs, carry):
+        for xx in range(X):
+            to_beside(zs, xx).wait_send()
+            to_mate(zs, xx).wait_send()
+            to_mate_again(zs, xx).wait_send()
+
+            @pl.when(jnp.logical_not(ends_here(zs, xx)))
+            def _():
+                home(zs, xx).wait_send()
+
+        return carry
+
+    lax.fori_loop(0, Z, drain, 0)
+
+
+def fused(S, T, L, activations, query_weight, key_weight, value_weight, out_weight, lambdas, head_gain):
+    R, D = activations.shape
+    X, Y = 2, 2
+    Z = S // Y
+    bf, f32 = jnp.bfloat16, jnp.float32
+    vmem = pl.BlockSpec(memory_space=pltpu.VMEM)
+    hbm = pl.BlockSpec(memory_space=pl.ANY)
+    smem = pl.BlockSpec(memory_space=pltpu.SMEM)
+    dma = pltpu.SemaphoreType.DMA
+    width = query_weight.shape[1]
+    return pl.pallas_call(
+        functools.partial(layer_kernel, S, T, L, R),
+        out_shape=jax.ShapeDtypeStruct((R, D), bf),
+        in_specs=[vmem, hbm, hbm, hbm, hbm, smem, vmem],
+        out_specs=vmem,
+        scratch_shapes=[
+            pltpu.VMEM((T, R, D), bf),
+            pltpu.VMEM((3, D, width), bf),
+            pltpu.VMEM((T * L, VALUE, D), bf),
+            pltpu.VMEM((L, X, 2, R, 768), bf),
+            pltpu.VMEM((Z, X, R, 768), bf),
+            pltpu.VMEM((S * T * R, 512), bf),
+            pltpu.VMEM((Z, X, R, VALUE), bf),
+            pltpu.VMEM((T * L, R, VALUE), bf),
+            pltpu.VMEM((L, 8, 128), f32),
+            pltpu.VMEM((L, 8, 128), f32),
+            pltpu.VMEM((Z, 2, X * R, VALUE), f32),
+            pltpu.VMEM((Z, 2, X * R, 128), f32),
+            pltpu.VMEM((Z, 2, X * R, 128), f32),
+            pltpu.VMEM((R, D), f32),
+            dma((3,)), dma((2,)),
+            dma((3,)), dma((T,)),
+            dma((1,)), dma((1,)),
+            dma((2 * L,)), dma((2 * L,)),
+            dma((2 * L + 1,)), dma((2 * L + 1,)),
+            dma((L, X, 2)), dma((Z, X)),
+            dma((3, Z, X)), dma((4, Z, X)),
+            dma((Z, X)), dma((T * L,)),
+        ],
+        compiler_params=pltpu.CompilerParams(
+            has_side_effects=True, vmem_limit_bytes=60 * 1024 * 1024
+        ),
+    )(
+        activations, query_weight, key_weight, value_weight,
+        out_weight.reshape(L, VALUE, D), lambdas, head_gain.reshape(1, VALUE),
+    )
 
 
 def empty_state(count, local_heads):
@@ -128,4 +542,15 @@
         P(),
     )
     out_specs = P(("sp", "tp"), None)
-    return jax.shard_map(shards, mesh=mesh, in_specs=in_specs, out_specs=out_specs, check_vma=False)
+    S, T = mesh.shape["sp"], mesh.shape["tp"]
+
+    def layer(*args):
+        L = args[5].shape[0] // T
+        rows = args[0].shape[0] // (S * T)
+        fits = T == 4 and L == 2 and S == L * T and rows % 16 == 0
+        local = functools.partial(fused, S, T, L) if fits else shards
+        return jax.shard_map(
+            local, mesh=mesh, in_specs=in_specs, out_specs=out_specs, check_vma=False
+        )(*args)
+
+    return layer

time: 277 us -> 79.3 us (0.29)
  waiting for transfers between devices: 193 us -> 0 us
  Pallas kernels: 0 us -> 77.3 us
  local copies, waits for them, and re-layouts: 32.1 us -> 1.82 us
  matrix products: 20.6 us -> 0 us
  between operations: 13.2 us -> 0.01 us
  other arithmetic: 10.4 us -> 0 us
  loops' own time: 5.22 us -> 0 us
    all_gather x3 -> x0, waiting for transfers between devices: 150 us -> none  [the longest x1 65 us: shards(): lax.all_gather(value_rows, 'sp', axis=0, tiled=True)]
    pallas_call x0 -> x1, Pallas kernels: none -> 77.3 us  [fused(): pl.pallas_call(functools.partial(layer_kernel, S, T, L, R), out_shape=jax...]
    reduce_scatter x1 -> x0, waiting for transfers between devices: 42.1 us -> none  [shards(): lax.psum_scatter(jnp.dot(heads_out, out_weight, preferred_element_type=jn...]
    dot_general x12 -> x0, matrix products: 20.6 us -> none  [the longest x5 7.46 us: absorb(): jnp.einsum('hmqk,khv->hmqv', exp_weights.astype(jnp.bfloat16), value_grid...]
    while x3 -> x0, local copies, waits for them, and re-layouts: 12 us -> none  [make_folder(): return lax.fori_loop(0, length // span, one_span, carry)]
    reduce_sum x6 -> x0, other arithmetic: 9.03 us -> none  [the longest x5 7.09 us: absorb(): denoms = denoms * factor + jnp.sum(exp_weights, axis=-1)]
    cond x25 -> x0, local copies, waits for them, and re-layouts: 6.52 us -> none
    dynamic_slice x5 -> x0, local copies, waits for them, and re-layouts: 6.4 us -> none  [one_span(): value_block = lax.dynamic_slice_in_dim(value_piece, offset, span, 0)]
  transfers between devices with their start and end apart: 4 -> 0, of which waited for: 4 -> 0; matrix products, arithmetic and copies ran while one was open for 2% -> 0% of each run, Pallas kernels for 0% -> 0%
where the time goes in v2:
time: 79.3 us; the launch traced here: 79.2 us
  Pallas kernels  77.3 us (97%)
  local copies, waits for them, and re-layouts  1.82 us (2%)
    pallas_call x1, Pallas kernels, fused(): pl.pallas_call(functools.partial(layer_kernel, S, T, L, R), out_shape=jax...  77.3 us
    unnamed x1, local copies, waits for them, and re-layouts  1.82 us

profile of v2, /device:TPU:16, one launch (start us, length us, event | category | flops | bytes accessed | tf_op | source)
XLA Modules:
  0.0 79.2 jit_solution(17613974230795882733)
XLA Ops:
  0.0 77.3 %shard_map.73 = bf16[112,2048]{1,0:T(8,128)(2,1)} custom-call(bf16[112,2048]{1,0:T(8,128)(2,1)} %act.1, bf16[2048,512]{1,0:T(8,128)(2,1)} %qw.1, bf16[2048,512]{1,0:T(8,128)(2,1)} %kw.1, bf16[2048,512]{1,0:T(8,128)(2,1)} %vw.1, bf16[2,256,2048]{2,1,0:T(8,128)(2,1)} %bitcast.2, f32[2]{0:T(128)} %lam_in.1, f32[1,256]{1,0:T(1,128)} %bitcast.3), custom_call_target="tpu_custom_call" | custom-call | tf_op jit(solution)/shard_map/pallas_call | solution.py:392
  77.3 1.8 %copy.9 = bf16[112,2048]{1,0:T(8,128)(2,1)} copy(bf16[112,2048]{1,0:T(8,128)(2,1)} %shard_map.73) | data formatting | bytes 917504

commit v3 on v2

--- a/solution.py
+++ b/solution.py
@@ -27,6 +27,7 @@
 ):
     X, Y = 2, 2
     Z = S // Y
+    H = Z // 2
     s = lax.axis_index("sp")
     t = lax.axis_index("tp")
     x = t // 2
@@ -88,10 +89,13 @@
 
     last = 2 * L - 1
 
-    def ow_beside():
-        place, rows = quarter(across, turn(0, y))
-        part = W.at[place, rows]
-        return remote(part, part, o_send.at[last], o_recv.at[last], beside, t)
+    cut = VALUE // 2 // (H * X)
+
+    def ow_beside(k, row):
+        q = turn(0, row)
+        first = pl.multiple_of((q % 2) * (VALUE // 2) + k * cut, cut)
+        part = W.at[across * L + q // 2, pl.ds(first, cut)]
+        return remote(part, part, o_send.at[last + k], o_recv.at[last + k], beside, t)
 
     def ow_pass(j):
         q = turn(0, 1 - y) if j == last else turn(j, y)
@@ -102,16 +106,26 @@
     def lam_out():
         return remote(LS, LB, lam_send.at[0], lam_recv.at[0], s, mate)
 
+    barrier = pltpu.get_barrier_semaphore()
+    greeted = [(beside, t)]
+    for i in range(Z):
+        row = ((z + i) % Z) * Y + y
+        greeted += [(row, mate), (row, across)] + ([(row, t)] if i > 0 else [])
+    for sp, tp in greeted:
+        pl.semaphore_signal(barrier, inc=1, device_id=(sp, tp), device_id_type=MESH)
+    weight_copies = [weight_copy(k) for k in range(3)]
+    for copy in weight_copies:
+        copy.start()
+    own_act().start()
+    own_ow().start()
+    pl.semaphore_wait(barrier, len(greeted))
+
     for l in range(L):
         LS[l] = jnp.full((8, 128), lam_in[l], jnp.float32)
     act_across().start()
     act_mate().start()
-    for k in range(3):
-        weight_copy(k).start()
-    own_act().start()
     for j in range(last):
         ow_across(j).start()
-    own_ow().start()
 
     def piece_sp(l):
         return (c * L + l) * Y + y
@@ -154,7 +168,6 @@
         weight_copy(k).wait()
     wait_act(mate)
     project(x)
-    ow_mate().start()
     lam_out().start()
     wait_act(across)
     act_pass().start()
@@ -203,9 +216,11 @@
         to_beside(zs, xx).wait_recv()
         to_mate_again(zs, xx).start()
 
-    def spread(first, count):
+    def spread(first, count, weights):
         def both(i, carry):
             forward(first + i)
+            if weights:
+                ow_beside(i, y).start()
 
             @pl.when(i > 0)
             def _():
@@ -287,11 +302,7 @@
     MX[...] = jnp.full(MX.shape, very_low, jnp.float32)
     DN[...] = jnp.zeros(DN.shape, jnp.float32)
     ACC[...] = jnp.zeros(ACC.shape, jnp.float32)
-    H = Z // 2
-    spread(0, H * X)
-    ow_across(0).wait_recv()
-    ow_beside().start()
-    ow_pass(0).start()
+    spread(0, H * X, False)
     lam_out().wait_recv()
     for i in range(H):
         wait_plane(near + i)
@@ -299,12 +310,23 @@
     def step(k, carry):
         @pl.when(k == H)
         def _():
-            spread(H * X, H * X)
+            ow_across(0).wait_recv()
+            spread(H * X, H * X, True)
+            ow_mate().start()
+            ow_pass(0).start()
             for i in range(H):
                 wait_plane((near + H + i) % Z)
             for j in range(1, last - 1):
                 ow_across(j).wait_recv()
                 ow_pass(j).start()
+
+        @pl.when(k == Z - 1)
+        def _():
+            ow_across(last - 1).wait_recv()
+            ow_pass(last - 1).start()
+            for i in range(H * X):
+                ow_beside(i, 1 - y).wait_recv()
+            ow_pass(last).start()
 
         early = k < H
         i = jnp.where(early, near + k, jnp.where(upper == 1, k - H, Z - 1 - (k - H)))
@@ -327,10 +349,6 @@
 
     own_ow().wait()
     ow_mate().wait_recv()
-    ow_across(last - 1).wait_recv()
-    ow_pass(last - 1).start()
-    ow_beside().wait_recv()
-    ow_pass(last).start()
     TOT[...] = jnp.zeros(TOT.shape, jnp.float32)
 
     def add_head(i, carry):
@@ -351,7 +369,8 @@
     act_mate().wait_send()
     act_pass().wait_send()
     ow_mate().wait_send()
-    ow_beside().wait_send()
+    for i in range(H * X):
+        ow_beside(i, y).wait_send()
     for j in range(last):
         ow_across(j).wait_send()
     for j in range(last + 1):
@@ -412,14 +431,14 @@
             dma((3,)), dma((2,)),
             dma((3,)), dma((T,)),
             dma((1,)), dma((1,)),
-            dma((2 * L,)), dma((2 * L,)),
+            dma((2 * L - 1 + Z // 2 * X,)), dma((2 * L - 1 + Z // 2 * X,)),
             dma((2 * L + 1,)), dma((2 * L + 1,)),
             dma((L, X, 2)), dma((Z, X)),
             dma((3, Z, X)), dma((4, Z, X)),
             dma((Z, X)), dma((T * L,)),
         ],
         compiler_params=pltpu.CompilerParams(
-            has_side_effects=True, vmem_limit_bytes=60 * 1024 * 1024
+            has_side_effects=True, collective_id=0, vmem_limit_bytes=60 * 1024 * 1024
         ),
     )(
         activations, query_weight, key_weight, value_weight,

time: 79.3 us -> 81.6 us (1.029)
  Pallas kernels: 77.3 us -> 79.3 us
    pallas_call x1, Pallas kernels: 77.3 us -> 79.3 us  [fused(): pl.pallas_call(functools.partial(layer_kernel, S, T, L, R), out_shape=jax...]
where the time goes in v3:
time: 81.6 us; the launch traced here: 81.2 us
  Pallas kernels  79.3 us (97%)
  local copies, waits for them, and re-layouts  1.82 us (2%)
    pallas_call x1, Pallas kernels, fused(): pl.pallas_call(functools.partial(layer_kernel, S, T, L, R), out_shape=jax...  79.3 us
    unnamed x1, local copies, waits for them, and re-layouts  1.82 us

profile of v3, /device:TPU:16, one launch (start us, length us, event | category | flops | bytes accessed | tf_op | source)
XLA Modules:
  0.0 81.2 jit_solution(8747645284415159872)
XLA Ops:
  0.0 79.3 %shard_map.73 = bf16[112,2048]{1,0:T(8,128)(2,1)} custom-call(bf16[112,2048]{1,0:T(8,128)(2,1)} %act.1, bf16[2048,512]{1,0:T(8,128)(2,1)} %qw.1, bf16[2048,512]{1,0:T(8,128)(2,1)} %kw.1, bf16[2048,512]{1,0:T(8,128)(2,1)} %vw.1, bf16[2,256,2048]{2,1,0:T(8,128)(2,1)} %bitcast.2, f32[2]{0:T(128)} %lam_in.1, f32[1,256]{1,0:T(1,128)} %bitcast.3), custom_call_target="tpu_custom_call" | custom-call | tf_op jit(solution)/shard_map/pallas_call | solution.py:411
  79.3 1.8 %copy.9 = bf16[112,2048]{1,0:T(8,128)(2,1)} copy(bf16[112,2048]{1,0:T(8,128)(2,1)} %shard_map.73) | data formatting | bytes 917504

commit v4 on v3

--- a/solution.py
+++ b/solution.py
@@ -89,7 +89,7 @@
 
     last = 2 * L - 1
 
-    cut = VALUE // 2 // (H * X)
+    cut = VALUE // 2 // H
 
     def ow_beside(k, row):
         q = turn(0, row)
@@ -202,7 +202,7 @@
         )
 
     def place(i):
-        return (near + i // X) % Z, (x + i) % X
+        return (near + i) % Z, (x + i // Z) % X
 
     def forward(i):
         zs, xx = place(i)
@@ -220,6 +220,10 @@
         def both(i, carry):
             forward(first + i)
             if weights:
+                @pl.when(i == 0)
+                def _():
+                    ow_across(0).wait_recv()
+
                 ow_beside(i, y).start()
 
             @pl.when(i > 0)
@@ -302,7 +306,7 @@
     MX[...] = jnp.full(MX.shape, very_low, jnp.float32)
     DN[...] = jnp.zeros(DN.shape, jnp.float32)
     ACC[...] = jnp.zeros(ACC.shape, jnp.float32)
-    spread(0, H * X, False)
+    spread(0, Z + H, False)
     lam_out().wait_recv()
     for i in range(H):
         wait_plane(near + i)
@@ -310,23 +314,17 @@
     def step(k, carry):
         @pl.when(k == H)
         def _():
-            ow_across(0).wait_recv()
-            spread(H * X, H * X, True)
+            spread(Z + H, H, True)
             ow_mate().start()
-            ow_pass(0).start()
             for i in range(H):
                 wait_plane((near + H + i) % Z)
+
+        @pl.when(k == Z - 1)
+        def _():
+            ow_pass(0).start()
             for j in range(1, last - 1):
                 ow_across(j).wait_recv()
                 ow_pass(j).start()
-
-        @pl.when(k == Z - 1)
-        def _():
-            ow_across(last - 1).wait_recv()
-            ow_pass(last - 1).start()
-            for i in range(H * X):
-                ow_beside(i, 1 - y).wait_recv()
-            ow_pass(last).start()
 
         early = k < H
         i = jnp.where(early, near + k, jnp.where(upper == 1, k - H, Z - 1 - (k - H)))
@@ -349,6 +347,11 @@
 
     own_ow().wait()
     ow_mate().wait_recv()
+    for i in range(H):
+        ow_beside(i, 1 - y).wait_recv()
+    ow_pass(last).start()
+    ow_across(last - 1).wait_recv()
+    ow_pass(last - 1).start()
     TOT[...] = jnp.zeros(TOT.shape, jnp.float32)
 
     def add_head(i, carry):
@@ -369,7 +372,7 @@
     act_mate().wait_send()
     act_pass().wait_send()
     ow_mate().wait_send()
-    for i in range(H * X):
+    for i in range(H):
         ow_beside(i, y).wait_send()
     for j in range(last):
         ow_across(j).wait_send()
@@ -431,7 +434,7 @@
             dma((3,)), dma((2,)),
             dma((3,)), dma((T,)),
             dma((1,)), dma((1,)),
-            dma((2 * L - 1 + Z // 2 * X,)), dma((2 * L - 1 + Z // 2 * X,)),
+            dma((2 * L - 1 + Z // 2,)), dma((2 * L - 1 + Z // 2,)),
             dma((2 * L + 1,)), dma((2 * L + 1,)),
             dma((L, X, 2)), dma((Z, X)),
             dma((3, Z, X)), dma((4, Z, X)),

time: 81.6 us -> 77.7 us (0.952)
  Pallas kernels: 79.3 us -> 75.4 us
    pallas_call x1, Pallas kernels: 79.3 us -> 75.4 us  [fused(): pl.pallas_call(functools.partial(layer_kernel, S, T, L, R), out_shape=jax...]
where the time goes in v4:
time: 77.7 us; the launch traced here: 77.2 us
  Pallas kernels  75.4 us (97%)
  local copies, waits for them, and re-layouts  1.82 us (2%)
    pallas_call x1, Pallas kernels, fused(): pl.pallas_call(functools.partial(layer_kernel, S, T, L, R), out_shape=jax...  75.4 us
    unnamed x1, local copies, waits for them, and re-layouts  1.82 us

profile of v4, /device:TPU:16, one launch (start us, length us, event | category | flops | bytes accessed | tf_op | source)
XLA Modules:
  0.0 77.2 jit_solution(1955944072952535446)
XLA Ops:
  0.0 75.4 %shard_map.73 = bf16[112,2048]{1,0:T(8,128)(2,1)} custom-call(bf16[112,2048]{1,0:T(8,128)(2,1)} %act.1, bf16[2048,512]{1,0:T(8,128)(2,1)} %qw.1, bf16[2048,512]{1,0:T(8,128)(2,1)} %kw.1, bf16[2048,512]{1,0:T(8,128)(2,1)} %vw.1, bf16[2,256,2048]{2,1,0:T(8,128)(2,1)} %bitcast.2, f32[2]{0:T(128)} %lam_in.1, f32[1,256]{1,0:T(1,128)} %bitcast.3), custom_call_target="tpu_custom_call" | custom-call | tf_op jit(solution)/shard_map/pallas_call | solution.py:414
  75.4 1.8 %copy.9 = bf16[112,2048]{1,0:T(8,128)(2,1)} copy(bf16[112,2048]{1,0:T(8,128)(2,1)} %shard_map.73) | data formatting | bytes 917504
